TPU v7x, 32 devices: a whole 2x2x4 slice. The times are simulated.
32 devices in a mesh: grp: 2 (over y), sp: 4 (over z), tp: 4 (over x, core).
Axes of the slice: x: 2, y: 2, z: 4, core: 2. Of those that a mesh axis runs over, the one named last changes fastest.
Arguments:
- tokens_in: bfloat16 [2048, 2048], P(('grp', 'sp'), 'tp'), parts along dimension 0, may hold values from -6 to 6
- norm_gain: float32 [3, 2048], replicated, may hold values from 0.1 to 1.9
- w_pool_in: bfloat16 [3, 2048, 1024], P(None, 'sp', 'tp'), may hold values from -0.125 to 0.125
- w_gate: bfloat16 [3, 2048, 2048], P(None, 'sp', 'tp'), may hold values from -0.125 to 0.125
- w_back: bfloat16 [3, 1024, 2048], P(None, 'tp', 'sp'), may hold values from -0.25 to 0.25
Outputs:
- tokens_out: bfloat16 [2048, 2048], P(('grp', 'sp'), 'tp'), parts along dimension 0
There are 2 independent parts, one for each index of `grp`. A program takes and returns all parts, laid end to end along the dimension named above; an argument that names none is the same for every part. Nothing has to cross between parts.
All inputs are finite; a program needn't handle non-finite values.
Results may differ from a plain program's by a relative error of at most 0.017.
Values may be sent and summed in bfloat16 or wider, within the bound.
A program may use at most 64 MiB of HBM per device.

v0:
```python
import jax
import jax.numpy as jnp
from jax import lax
from jax.sharding import PartitionSpec as P

POOL_WIDTH = 1024
GROUPS = 4
GRID_W = 32
LAYERS = 3


pool_windows = (2, 4, 8, 16)
norm_eps = 1e-06


def padded_2(value, sides, width):
    for axis, dim in sides:
        peers, length = (lax.axis_size(axis), value.shape[dim])
        up = [(i, (i + 1) % peers) for i in range(peers - 1)]
        down = [(j, i) for i, j in up]
        last = lax.slice_in_dim(value, length - width, length, axis=dim)
        initial = lax.slice_in_dim(value, 0, width, axis=dim)
        before = lax.ppermute(last, axis, up)
        after = lax.ppermute(initial, axis, down)
        value = jnp.concatenate([before, value, after], axis=dim)
    return value


def window_means(padded, rows_here, first_row, total_rows, window):
    reach = max(pool_windows) // 2
    half_span = window // 2
    width_cols = padded.shape[1] - 2 * reach
    row_sums = padded[reach - half_span : reach - half_span + rows_here]
    for offset in range(1 - half_span, half_span):
        row_sums = row_sums + padded[reach + offset : reach + offset + rows_here]
    box_sums = row_sums[:, reach - half_span : reach - half_span + width_cols]
    for offset in range(1 - half_span, half_span):
        box_sums = box_sums + row_sums[:, reach + offset : reach + offset + width_cols]
    row_index = first_row + jnp.arange(rows_here, dtype=jnp.int32)
    col_index = jnp.arange(width_cols, dtype=jnp.int32)
    row_counts = jnp.minimum(row_index + half_span, total_rows) - jnp.maximum(
        row_index - half_span, 0
    )
    col_counts = jnp.minimum(col_index + half_span, width_cols) - jnp.maximum(
        col_index - half_span, 0
    )
    counts = (row_counts[:, None] * col_counts[None, :]).astype(jnp.float32)
    return box_sums / counts[:, :, None]


def on_device(tokens_in, norm_gain, w_pool_in, w_gate, w_back):
    reach = max(pool_windows) // 2
    sp_count = lax.axis_size("sp")
    tp_count = lax.axis_size("tp")
    tp_pos = lax.axis_index("tp")
    sp_pos = lax.axis_index("sp")
    tok_rows = tokens_in.shape[0]
    rows_here = tok_rows // GRID_W
    total_rows = rows_here * sp_count
    first_row = sp_pos * rows_here
    local_pool = w_pool_in.shape[2]
    group_width = POOL_WIDTH // GROUPS
    channel_group = (tp_pos * local_pool + jnp.arange(local_pool, dtype=jnp.int32)) // group_width
    state = tokens_in
    for layer_id in range(LAYERS):
        whole_rows = lax.all_gather(state, "tp", axis=1, tiled=True)
        wide = whole_rows.astype(jnp.float32)
        normed = (
            wide
            * lax.rsqrt(jnp.mean(wide * wide, axis=-1, keepdims=True) + norm_eps)
            * norm_gain[layer_id]
        ).astype(jnp.bfloat16)
        pool_acc = jnp.dot(
            normed,
            lax.all_gather(w_pool_in[layer_id], "sp", axis=0, tiled=True),
            preferred_element_type=jnp.float32,
        )
        gate_acc = jnp.dot(
            normed,
            lax.all_gather(w_gate[layer_id], "sp", axis=0, tiled=True),
            preferred_element_type=jnp.float32,
        )
        pool_in = pool_acc.astype(jnp.bfloat16)
        gate = jax.nn.sigmoid(gate_acc)
        cells = pool_in.reshape(rows_here, GRID_W, local_pool)
        rimmed = padded_2(cells, (("sp", 0),), reach)
        padded = jnp.pad(rimmed.astype(jnp.float32), ((0, 0), (reach, reach), (0, 0)))
        means = jnp.zeros((rows_here, GRID_W, local_pool), jnp.float32)
        for group_id in range(GROUPS):
            in_group = (channel_group == group_id)[None, None, :]
            means = jnp.where(
                in_group,
                window_means(padded, rows_here, first_row, total_rows, pool_windows[group_id]),
                means,
            )
        pooled = (
            (means - cells.astype(jnp.float32)).reshape(tok_rows, local_pool).astype(jnp.bfloat16)
        )
        full_pooled = lax.all_gather(pooled, "tp", axis=1, tiled=True)
        back_rows = lax.all_gather(w_back[layer_id], "sp", axis=1, tiled=True)
        back_cols = lax.all_to_all(back_rows, "tp", split_axis=1, concat_axis=0, tiled=True)
        partials = jnp.einsum(
            "tnb,nbd->ntd",
            full_pooled.reshape(tok_rows, tp_count, local_pool),
            back_cols.reshape(tp_count, local_pool, back_cols.shape[1]),
            preferred_element_type=jnp.float32,
        ).astype(jnp.bfloat16)
        branch = jnp.sum(partials.astype(jnp.float32), axis=0)
        state = (state.astype(jnp.float32) + gate * branch).astype(jnp.bfloat16)
    return state


def solution(mesh):
    return jax.shard_map(
        on_device,
        mesh=mesh,
        in_specs=(
            P(("grp", "sp"), "tp"),
            P(),
            P(None, "sp", "tp"),
            P(None, "sp", "tp"),
            P(None, "tp", "sp"),
        ),
        out_specs=P(("grp", "sp"), "tp"),
        check_vma=False,
    )
```

profile of v0, /device:TPU:0, one launch (start us, length us, event | category | flops | bytes accessed | tf_op | source)
XLA Modules:
  0.0 391.0 jit_solution(7945444731493379469)
XLA Ops:
  6.5 0.7 all-gather.22.cloned.1.call-update
  7.3 2.2 fusion.168
  9.6 0.8 fusion.167
  10.3 0.8 copy.33
  11.3 1.2 fusion.166
  12.9 0.6 fusion.169
  13.5 14.9 %all-gather.22.cloned.1.call-done = bf16[256,2048]{1,0:T(8,128)(2,1)} async-done(((bf16[256,512]{1,0:T(8,128)(2,1)}), bf16[256,2048]{1,0:T(8,128)(2,1)}) %all-gather.22.cloned.1.call-update) | async-done | bytes 1048592 | tf_op jit(solution)/shard_map/all_gather | solution.py:66
  28.3 1.5 fusion
  29.9 28.1 %all-gather.30.cloned.1.call-done = bf16[1,2048,256]{2,1,0:T(8,128)(2,1)} async-done(((bf16[1,512,256]{2,1,0:T(8,128)(2,1)}), bf16[1,2048,256]{2,1,0:T(8,128)(2,1)}) %all-gather.30.cloned.1.call-update) | async-done | bytes 1048592 | tf_op jit(solution)/shard_map/all_gather | solution.py:75
  57.9 2.0 convolution_convert_fusion.5
  60.0 3.4 collective-permute-start
  63.3 1.3 collective-permute-start.1
  64.7 23.0 %all-gather.32.cloned.1.call-done = bf16[1,256,2048]{1,2,0:T(8,128)(2,1)} async-done(((bf16[1,256,512]{1,2,0:T(8,128)(2,1)}), bf16[1,256,2048]{1,2,0:T(8,128)(2,1)}) %all-gather.32.cloned.1.call-update) | async-done | bytes 1048592 | tf_op jit(solution)/shard_map/all_gather | solution.py:100
  87.7 2.3 copy.20
  90.0 3.5 all-to-all-start
  94.1 0.8 fusion.151
  94.9 16.6 %all_gather.48 = bf16[256,1024]{1,0:T(8,128)(2,1)S(1)} all-gather(bf16[256,256]{1,0:T(8,128)(2,1)S(1)} %bitcast.112), channel_id=1, replica_groups=mesh['grp'=2,'sp'=4,'tp'=4] {'tp'}, dimensions={1}, use_global_device_ids=true | all-gather | bytes 655360 | tf_op jit(solution)/shard_map/all_gather | solution.py:99
  112.3 21.1 %all-gather.28.cloned.1.call-done = bf16[1,2048,512]{2,1,0:T(8,128)(2,1)} async-done(((bf16[1,512,512]{2,1,0:T(8,128)(2,1)}), bf16[1,2048,512]{2,1,0:T(8,128)(2,1)}) %all-gather.28.cloned.1.call-update) | async-done | bytes 2097168 | tf_op jit(solution)/shard_map/all_gather | solution.py:80
  133.4 3.2 fusion.75
  137.2 0.8 copy.34
  138.1 0.7 all-gather.34.cloned.1.call-update
  138.8 13.4 %all-gather.24.cloned.1.call-done = bf16[256,2048]{1,0:T(8,128)(2,1)} async-done(((bf16[256,512]{1,0:T(8,128)(2,1)}), bf16[256,2048]{1,0:T(8,128)(2,1)}) %all-gather.24.cloned.1.call-update) | async-done | bytes 1048592 | tf_op jit(solution)/shard_map/all_gather | solution.py:66
  152.2 1.5 fusion.3
  153.8 27.9 %all-gather.36.cloned.1.call-done = bf16[1,2048,256]{2,1,0:T(8,128)(2,1)} async-done(((bf16[1,512,256]{2,1,0:T(8,128)(2,1)}), bf16[1,2048,256]{2,1,0:T(8,128)(2,1)}) %all-gather.36.cloned.1.call-update) | async-done | bytes 1048592 | tf_op jit(solution)/shard_map/all_gather | solution.py:75
  181.7 2.0 convolution_convert_fusion.4
  183.7 3.4 collective-permute-start.2
  187.1 1.3 collective-permute-start.3
  188.4 23.1 %all-gather.38.cloned.1.call-done = bf16[1,256,2048]{1,2,0:T(8,128)(2,1)} async-done(((bf16[1,256,512]{1,2,0:T(8,128)(2,1)}), bf16[1,256,2048]{1,2,0:T(8,128)(2,1)}) %all-gather.38.cloned.1.call-update) | async-done | bytes 1048592 | tf_op jit(solution)/shard_map/all_gather | solution.py:100
  211.5 2.3 copy.24
  213.7 3.5 all-to-all-start.1
  218.4 0.8 fusion.152
  219.2 16.1 %all_gather.53 = bf16[256,1024]{1,0:T(8,128)(2,1)S(1)} all-gather(bf16[256,256]{1,0:T(8,128)(2,1)S(1)} %bitcast.113), channel_id=1, replica_groups=mesh['grp'=2,'sp'=4,'tp'=4] {'tp'}, dimensions={1}, use_global_device_ids=true | all-gather | bytes 655360 | tf_op jit(solution)/shard_map/all_gather | solution.py:99
  236.0 21.2 %all-gather.34.cloned.1.call-done = bf16[1,2048,512]{2,1,0:T(8,128)(2,1)} async-done(((bf16[1,512,512]{2,1,0:T(8,128)(2,1)}), bf16[1,2048,512]{2,1,0:T(8,128)(2,1)}) %all-gather.34.cloned.1.call-update) | async-done | bytes 2097168 | tf_op jit(solution)/shard_map/all_gather | solution.py:80
  257.3 3.1 fusion.72
  261.1 0.8 copy.35
  262.5 13.6 %all-gather.26.cloned.1.call-done = bf16[256,2048]{1,0:T(8,128)(2,1)} async-done(((bf16[256,512]{1,0:T(8,128)(2,1)}), bf16[256,2048]{1,0:T(8,128)(2,1)}) %all-gather.26.cloned.1.call-update) | async-done | bytes 1048592 | tf_op jit(solution)/shard_map/all_gather | solution.py:66
  276.1 1.5 fusion.6
  277.6 27.9 %all-gather.42.cloned.1.call-done = bf16[1,2048,256]{2,1,0:T(8,128)(2,1)} async-done(((bf16[1,512,256]{2,1,0:T(8,128)(2,1)}), bf16[1,2048,256]{2,1,0:T(8,128)(2,1)}) %all-gather.42.cloned.1.call-update) | async-done | bytes 1048592 | tf_op jit(solution)/shard_map/all_gather | solution.py:75
  305.5 2.0 convolution_convert_fusion.3
  307.6 3.4 collective-permute-start.4
  310.9 1.3 collective-permute-start.5
  312.2 23.1 %all-gather.44.cloned.1.call-done = bf16[1,256,2048]{1,2,0:T(8,128)(2,1)} async-done(((bf16[1,256,512]{1,2,0:T(8,128)(2,1)}), bf16[1,256,2048]{1,2,0:T(8,128)(2,1)}) %all-gather.44.cloned.1.call-update) | async-done | bytes 1048592 | tf_op jit(solution)/shard_map/all_gather | solution.py:100
  335.3 2.3 copy.28
  337.6 3.7 all-to-all-start.2
  342.3 0.8 fusion.153
  343.1 16.1 %all_gather.58 = bf16[256,1024]{1,0:T(8,128)(2,1)S(1)} all-gather(bf16[256,256]{1,0:T(8,128)(2,1)S(1)} %bitcast.111), channel_id=1, replica_groups=mesh['grp'=2,'sp'=4,'tp'=4] {'tp'}, dimensions={1}, use_global_device_ids=true | all-gather | bytes 655360 | tf_op jit(solution)/shard_map/all_gather | solution.py:99
  359.9 21.1 %all-gather.40.cloned.1.call-done = bf16[1,2048,512]{2,1,0:T(8,128)(2,1)} async-done(((bf16[1,512,512]{2,1,0:T(8,128)(2,1)}), bf16[1,2048,512]{2,1,0:T(8,128)(2,1)}) %all-gather.40.cloned.1.call-update) | async-done | bytes 2097168 | tf_op jit(solution)/shard_map/all_gather | solution.py:80
  381.0 3.1 fusion.69
  (113 shorter events, 7.0 us)
Async XLA Ops:
  6.5 3.0 copy-start.5
  6.5 21.8 %all-gather.22.cloned.1.call-start = ((), (), s32[]{:S(2)}) async-start(), calls=%async_computation.3 | async-start | bytes 1310720 | tf_op jit(solution)/shard_map/all_gather | solution.py:66
  7.3 4.0 %copy-start = (bf16[3,512,512]{2,1,0:T(8,128)(2,1)S(1)}, bf16[3,512,512]{2,1,0:T(8,128)(2,1)}, u32[]{:S(2)}) copy-start(bf16[3,512,512]{2,1,0:T(8,128)(2,1)} %param.8) | copy-start | bytes 4718596
  7.3 50.7 %all-gather.30.cloned.1.call-start = ((), (), s32[]{:S(2)}) async-start(), calls=%async_computation.7 | async-start | bytes 1310720 | tf_op jit(solution)/shard_map/all_gather | solution.py:75
  9.5 78.2 %all-gather.32.cloned.1.call-start = ((), (), s32[]{:S(2)}) async-start(), calls=%async_computation.8 | async-start | bytes 1310720 | tf_op jit(solution)/shard_map/all_gather | solution.py:100
  11.2 1.7 copy-start.6
  11.2 122.2 %all-gather.28.cloned.1.call-start = ((), (), s32[]{:S(2)}) async-start(), calls=%async_computation.6 | async-start | bytes 2621440 | tf_op jit(solution)/shard_map/all_gather | solution.py:80
  13.5 46.5 %copy-start.10 = (f32[1,2048]{1,0:T(1,128)}, f32[1,2048]{1,0:T(1,128)S(1)}, u32[]{:S(2)}) copy-start(f32[1,2048]{1,0:T(1,128)S(1)} %get-tuple-element.27) | copy-start | bytes 24580
  29.9 60.1 %copy-start.23 = (f32[256]{0:T(256)}, f32[256]{0:T(256)S(1)}, u32[]{:S(2)}) copy-start(f32[256]{0:T(256)S(1)} %add_rsqrt_fusion.2) | copy-start | bytes 3076
  60.0 33.6 %collective-permute-start = (bf16[8,32,256]{2,1,0:T(8,128)(2,1)S(1)}, bf16[8,32,256]{2,1,0:T(8,128)(2,1)S(1)}, u32[]{:S(2)}, u32[]{:S(2)}) collective-permute-start(bf16[8,32,256]{2,1,0:T(8,128)(2,1)S(1)} %bitcast.99), channel_id=1, source_target_pairs={{0,4},{4,8},{8,12},{1,5},{5,9},{9,13},{2,6},{6,10},{10,14},{3,7},{... | collective-permute-start | bytes 393224 | tf_op jit(solution)/shard_map/ppermute | solution.py:23
  63.3 30.2 %collective-permute-start.1 = (bf16[8,32,256]{2,1,0:T(8,128)(2,1)S(1)}, bf16[8,32,256]{2,1,0:T(8,128)(2,1)S(1)}, u32[]{:S(2)}, u32[]{:S(2)}) collective-permute-start(bf16[8,32,256]{2,1,0:T(8,128)(2,1)S(1)} %bitcast.100), channel_id=1, source_target_pairs={{4,0},{8,4},{12,8},{5,1},{9,5},{13,9},{6,2},{10,6},{14,10},{7,3},{... | collective-permute-start | bytes 393224 | tf_op jit(solution)/shard_map/ppermute | solution.py:24
  64.7 29.4 %copy-start.11 = (pred[256]{0:T(512)(128)(4,1)}, pred[256]{0:T(512)(128)(4,1)S(1)}, u32[]{:S(2)}) copy-start(pred[256]{0:T(512)(128)(4,1)S(1)} %get-tuple-element.33) | copy-start | bytes 772
  64.7 29.4 %copy-start.14 = (pred[256]{0:T(512)(128)(4,1)}, pred[256]{0:T(512)(128)(4,1)S(1)}, u32[]{:S(2)}) copy-start(pred[256]{0:T(512)(128)(4,1)S(1)} %get-tuple-element.34) | copy-start | bytes 772
  64.7 29.4 %copy-start.17 = (pred[256]{0:T(512)(128)(4,1)}, pred[256]{0:T(512)(128)(4,1)S(1)}, u32[]{:S(2)}) copy-start(pred[256]{0:T(512)(128)(4,1)S(1)} %get-tuple-element.35) | copy-start | bytes 772
  64.7 29.4 %copy-start.20 = (pred[256]{0:T(512)(128)(4,1)}, pred[256]{0:T(512)(128)(4,1)S(1)}, u32[]{:S(2)}) copy-start(pred[256]{0:T(512)(128)(4,1)S(1)} %get-tuple-element.36) | copy-start | bytes 772
  90.0 21.8 %all-to-all-start = ((bf16[256,4,512]{2,0,1:T(8,128)(2,1)}), bf16[256,4,512]{2,0,1:T(8,128)(2,1)S(1)}, u32[]{:S(2)}, u32[]{:S(2)}) async-start(bf16[256,4,512]{2,0,1:T(8,128)(2,1)} %copy.20), calls=%async_computation | async-start | bytes 2097152 | tf_op jit(solution)/shard_map/all_to_all | solution.py:101
  93.5 58.7 %all-gather.24.cloned.1.call-start = ((), (), s32[]{:S(2)}) async-start(), calls=%async_computation.4 | async-start | bytes 1310720 | tf_op jit(solution)/shard_map/all_gather | solution.py:66
  94.9 38.5 %copy-start.1 = (bf16[256,2048]{1,0:T(8,128)(2,1)S(1)}, bf16[256,2048]{1,0:T(8,128)(2,1)}, u32[]{:S(2)}) copy-start(bf16[256,2048]{1,0:T(8,128)(2,1)} %all-gather.22.cloned.1.call-done) | copy-start | bytes 3145732
  112.3 24.9 %copy-start.4 = (bf16[1,256,512]{2,1,0:T(8,128)(2,1)S(1)}, bf16[1,256,512]{2,1,0:T(8,128)(2,1)}, u32[]{:S(2)}) copy-start(bf16[1,256,512]{2,1,0:T(8,128)(2,1)} %get-tuple-element.21) | copy-start | bytes 786436
  136.5 45.1 %copy-start.8 = (f32[1,2048]{1,0:T(1,128)S(1)}, f32[1,2048]{1,0:T(1,128)}, u32[]{:S(2)}) copy-start(f32[1,2048]{1,0:T(1,128)} %get-tuple-element.28) | copy-start | bytes 24580
  136.6 45.1 %all-gather.36.cloned.1.call-start = ((), (), s32[]{:S(2)}) async-start(), calls=%async_computation.10 | async-start | bytes 1310720 | tf_op jit(solution)/shard_map/all_gather | solution.py:75
  137.1 74.3 %all-gather.38.cloned.1.call-start = ((), (), s32[]{:S(2)}) async-start(), calls=%async_computation.11 | async-start | bytes 1310720 | tf_op jit(solution)/shard_map/all_gather | solution.py:100
  138.1 119.2 %all-gather.34.cloned.1.call-start = ((), (), s32[]{:S(2)}) async-start(), calls=%async_computation.9 | async-start | bytes 2621440 | tf_op jit(solution)/shard_map/all_gather | solution.py:80
  153.8 60.0 %copy-start.24 = (f32[256]{0:T(256)}, f32[256]{0:T(256)S(1)}, u32[]{:S(2)}) copy-start(f32[256]{0:T(256)S(1)} %add_rsqrt_fusion.1) | copy-start | bytes 3076
  183.7 33.6 %collective-permute-start.2 = (bf16[8,32,256]{2,1,0:T(8,128)(2,1)S(1)}, bf16[8,32,256]{2,1,0:T(8,128)(2,1)S(1)}, u32[]{:S(2)}, u32[]{:S(2)}) collective-permute-start(bf16[8,32,256]{2,1,0:T(8,128)(2,1)S(1)} %bitcast.107), channel_id=1, source_target_pairs={{0,4},{4,8},{8,12},{1,5},{5,9},{9,13},{2,6},{6,10},{10,14},{3,7},{... | collective-permute-start | bytes 393224 | tf_op jit(solution)/shard_map/ppermute | solution.py:23
  187.1 30.3 %collective-permute-start.3 = (bf16[8,32,256]{2,1,0:T(8,128)(2,1)S(1)}, bf16[8,32,256]{2,1,0:T(8,128)(2,1)S(1)}, u32[]{:S(2)}, u32[]{:S(2)}) collective-permute-start(bf16[8,32,256]{2,1,0:T(8,128)(2,1)S(1)} %bitcast.108), channel_id=1, source_target_pairs={{4,0},{8,4},{12,8},{5,1},{9,5},{13,9},{6,2},{10,6},{14,10},{7,3},{... | collective-permute-start | bytes 393224 | tf_op jit(solution)/shard_map/ppermute | solution.py:24
  213.7 21.8 %all-to-all-start.1 = ((bf16[256,4,512]{2,0,1:T(8,128)(2,1)}), bf16[256,4,512]{2,0,1:T(8,128)(2,1)S(1)}, u32[]{:S(2)}, u32[]{:S(2)}) async-start(bf16[256,4,512]{2,0,1:T(8,128)(2,1)} %copy.24), calls=%async_computation.1 | async-start | bytes 2097152 | tf_op jit(solution)/shard_map/all_to_all | solution.py:101
  217.3 58.8 %all-gather.26.cloned.1.call-start = ((), (), s32[]{:S(2)}) async-start(), calls=%async_computation.5 | async-start | bytes 1310720 | tf_op jit(solution)/shard_map/all_gather | solution.py:66
  217.7 0.6 copy-start.12
  217.7 0.6 copy-start.15
  217.7 0.7 copy-start.18
  217.7 0.7 copy-start.21
  219.2 38.1 %copy-start.3 = (bf16[256,2048]{1,0:T(8,128)(2,1)S(1)}, bf16[256,2048]{1,0:T(8,128)(2,1)}, u32[]{:S(2)}) copy-start(bf16[256,2048]{1,0:T(8,128)(2,1)} %all-gather.24.cloned.1.call-done) | copy-start | bytes 3145732
  219.2 38.0 %copy-start.9 = (f32[1,2048]{1,0:T(1,128)S(1)}, f32[1,2048]{1,0:T(1,128)}, u32[]{:S(2)}) copy-start(f32[1,2048]{1,0:T(1,128)} %get-tuple-element.28) | copy-start | bytes 24580
  219.2 38.0 %copy-start.25 = (f32[256]{0:T(256)S(1)}, f32[256]{0:T(256)}, u32[]{:S(2)}) copy-start(f32[256]{0:T(256)} %copy-done.24) | copy-start | bytes 3076
  260.4 45.1 %copy-start.7 = (f32[1,2048]{1,0:T(1,128)S(1)}, f32[1,2048]{1,0:T(1,128)}, u32[]{:S(2)}) copy-start(f32[1,2048]{1,0:T(1,128)} %get-tuple-element.26) | copy-start | bytes 24580
  260.4 45.1 %all-gather.42.cloned.1.call-start = ((), (), s32[]{:S(2)}) async-start(), calls=%async_computation.13 | async-start | bytes 1310720 | tf_op jit(solution)/shard_map/all_gather | solution.py:75
  261.0 74.3 %all-gather.44.cloned.1.call-start = ((), (), s32[]{:S(2)}) async-start(), calls=%async_computation.14 | async-start | bytes 1310720 | tf_op jit(solution)/shard_map/all_gather | solution.py:100
  261.9 119.0 %all-gather.40.cloned.1.call-start = ((), (), s32[]{:S(2)}) async-start(), calls=%async_computation.12 | async-start | bytes 2621440 | tf_op jit(solution)/shard_map/all_gather | solution.py:80
  307.6 33.7 %collective-permute-start.4 = (bf16[8,32,256]{2,1,0:T(8,128)(2,1)S(1)}, bf16[8,32,256]{2,1,0:T(8,128)(2,1)S(1)}, u32[]{:S(2)}, u32[]{:S(2)}) collective-permute-start(bf16[8,32,256]{2,1,0:T(8,128)(2,1)S(1)} %bitcast.103), channel_id=1, source_target_pairs={{0,4},{4,8},{8,12},{1,5},{5,9},{9,13},{2,6},{6,10},{10,14},{3,7},{... | collective-permute-start | bytes 393224 | tf_op jit(solution)/shard_map/ppermute | solution.py:23
  310.9 30.4 %collective-permute-start.5 = (bf16[8,32,256]{2,1,0:T(8,128)(2,1)S(1)}, bf16[8,32,256]{2,1,0:T(8,128)(2,1)S(1)}, u32[]{:S(2)}, u32[]{:S(2)}) collective-permute-start(bf16[8,32,256]{2,1,0:T(8,128)(2,1)S(1)} %bitcast.104), channel_id=1, source_target_pairs={{4,0},{8,4},{12,8},{5,1},{9,5},{13,9},{6,2},{10,6},{14,10},{7,3},{... | collective-permute-start | bytes 393224 | tf_op jit(solution)/shard_map/ppermute | solution.py:24
  337.6 21.8 %all-to-all-start.2 = ((bf16[256,4,512]{2,0,1:T(8,128)(2,1)}), bf16[256,4,512]{2,0,1:T(8,128)(2,1)S(1)}, u32[]{:S(2)}, u32[]{:S(2)}) async-start(bf16[256,4,512]{2,0,1:T(8,128)(2,1)} %copy.28), calls=%async_computation.2 | async-start | bytes 2097152 | tf_op jit(solution)/shard_map/all_to_all | solution.py:101
  341.6 0.6 copy-start.13
  341.6 0.6 copy-start.16
  341.6 0.7 copy-start.19
  341.6 0.7 copy-start.22
  343.1 37.9 %copy-start.2 = (bf16[256,2048]{1,0:T(8,128)(2,1)S(1)}, bf16[256,2048]{1,0:T(8,128)(2,1)}, u32[]{:S(2)}) copy-start(bf16[256,2048]{1,0:T(8,128)(2,1)} %all-gather.26.cloned.1.call-done) | copy-start | bytes 3145732
Sparse Core Ops, SparseCore 0:
  8.9 19.4 all-gather.21
  29.9 27.9 all-gather.29
  59.5 28.1 all-gather.31
  89.1 44.1 all-gather.27
  136.7 15.4 all-gather.23
  153.7 27.9 all-gather.35
  183.2 28.1 all-gather.37
  213.0 44.1 all-gather.33
  260.6 15.4 all-gather.25
  277.5 27.9 all-gather.41
  307.1 28.1 all-gather.43
  336.7 44.2 all-gather.39
where the time goes:
time: 392 us; the launch traced here: 391 us
  waiting for transfers between devices  261 us (67%)
  blocking collectives  48.8 us (12%)
  starting transfers between devices  25.1 us (6%)
  matrix products  16.9 us (4%)
  local copies, waits for them, and re-layouts  15.8 us (4%)
  between operations  14.2 us (4%)
  other arithmetic  8.76 us (2%)
    all_gather x3, waiting for transfers between devices, on_device(): lax.all_gather(w_pool_in[layer_id], 'sp', axis=0, tiled=True)  83.9 us
    all_gather x3, waiting for transfers between devices, on_device(): back_rows = lax.all_gather(w_back[layer_id], 'sp', axis=1, tiled=True)  69.2 us
    all_gather x3, waiting for transfers between devices, on_device(): lax.all_gather(w_gate[layer_id], 'sp', axis=0, tiled=True)  63.4 us
    all_gather x3, blocking collectives, on_device(): full_pooled = lax.all_gather(pooled, 'tp', axis=1, tiled=True)  48.8 us
    all_gather x3, waiting for transfers between devices, on_device(): whole_rows = lax.all_gather(state, 'tp', axis=1, tiled=True)  41.8 us
    all_to_all x3, starting transfers between devices, on_device(): lax.all_to_all(back_rows, 'tp', split_axis=1, concat_axis=0, tiled=True)  10.7 us
    ppermute x3, starting transfers between devices, padded_2(): before = lax.ppermute(last, axis, up)  10.1 us
    dot_general x3, matrix products, on_device(): jnp.dot(normed, lax.all_gather(w_gate[layer_id], 'sp', axis=0, tiled=True...  9.41 us
  transfers between devices with their start and end apart: 21, of which 12 were waited for; matrix products, arithmetic and copies ran while one was open for 8% of the time, Pallas kernels for 0%

commit v1 on v0

--- a/solution.py
+++ b/solution.py
@@ -1,7 +1,10 @@
 import jax
 import jax.numpy as jnp
 from jax import lax
+from jax.experimental import pallas as pl
+from jax.experimental.pallas import tpu as pltpu
 from jax.sharding import PartitionSpec as P
+import functools
 
 POOL_WIDTH = 1024
 GROUPS = 4
@@ -110,9 +113,378 @@
     return state
 
 
+MESH = pl.DeviceIdType.MESH
+
+
+def halves(buffers, layer, block, half):
+    views = []
+    for buf in buffers:
+        rows = buf.shape[2] // 2
+        views.append(buf.at[layer, block, pl.ds(pl.multiple_of(half * rows, rows), rows), :])
+    return views
+
+
+def fused_kernel(
+    sp_count, tp_count,
+    tok_hbm, gain_ref, wp_hbm, wg_hbm, wb_hbm, out_ref,
+    wp, wg, wb, gathered, normed, halo, gate_buf, box, counts, parts, arrived,
+    load_sem, z_send, z_recv, y_send, y_recv, ag_send, ag_recv, h_send, h_recv, rs_send, rs_recv,
+):
+    g = lax.axis_index("grp")
+    s = lax.axis_index("sp")
+    t = lax.axis_index("tp")
+    other = 1 - g
+    t1 = t + 1 - 2 * (t % 2)
+    t2 = (t + 2) % tp_count
+    t3 = (t1 + 2) % tp_count
+    last = sp_count - 1
+    toks, feats = tok_hbm.shape
+    rows_here = toks // GRID_W
+    total_rows = rows_here * sp_count
+    weights = (wp, wg, wb)
+    sources = (wp_hbm, wg_hbm, wb_hbm)
+    rounds = sp_count - 1
+
+    def load(layer, piece):
+        return pltpu.make_async_copy(
+            sources[piece].at[layer], weights[piece].at[layer, s], load_sem.at[layer, piece]
+        )
+
+    state_load = pltpu.make_async_copy(tok_hbm, gathered.at[0, t], load_sem.at[LAYERS, 0])
+    state_load.start()
+    for piece in range(3):
+        load(0, piece).start()
+    for layer in range(1, LAYERS):
+        for piece in range(3):
+            load(layer, piece).start()
+
+    barrier = pltpu.get_barrier_semaphore()
+    for target in ({"grp": other}, {"tp": t1}, {"tp": t2}, {"tp": t3}):
+        pl.semaphore_signal(barrier, inc=1, device_id=target, device_id_type=MESH)
+
+    @pl.when(s > 0)
+    def _():
+        pl.semaphore_signal(barrier, inc=1, device_id={"sp": s - 1}, device_id_type=MESH)
+
+    @pl.when(s < last)
+    def _():
+        pl.semaphore_signal(barrier, inc=1, device_id={"sp": s + 1}, device_id_type=MESH)
+
+    pl.semaphore_wait(barrier, 4 + jnp.where(s > 0, 1, 0) + jnp.where(s < last, 1, 0))
+
+    def sent_block(way, k):
+        return s - k if way == 0 else s + k
+
+    def got_block(way, k):
+        return s - 1 - k if way == 0 else s + 1 + k
+
+    def gets(way, k):
+        return s - 1 - k >= 0 if way == 0 else s + 1 + k <= last
+
+    def sends(way, k):
+        if way == 0:
+            return jnp.logical_and(s - k >= 0, s < last)
+        return jnp.logical_and(s + k <= last, s > 0)
+
+    def z_copy(layer, way, k, piece, block):
+        view = halves(weights, layer, block, g)[piece]
+        return pltpu.make_async_remote_copy(
+            src_ref=view, dst_ref=view,
+            send_sem=z_send.at[layer, way, k, piece], recv_sem=z_recv.at[layer, way, k, piece],
+            device_id={"sp": s + 1 if way == 0 else s - 1}, device_id_type=MESH,
+        )
+
+    def y_copy(layer, way, k, piece, half):
+        view = halves(weights, layer, got_block(way, k), half)[piece]
+        return pltpu.make_async_remote_copy(
+            src_ref=view, dst_ref=view,
+            send_sem=y_send.at[layer, way, k, piece], recv_sem=y_recv.at[layer, way, k, piece],
+            device_id={"grp": other}, device_id_type=MESH,
+        )
+
+    def own_sends(layer):
+        for piece in range(3):
+            load(layer, piece).wait()
+            for way in range(2):
+                @pl.when(sends(way, 0))
+                def _(way=way, piece=piece):
+                    z_copy(layer, way, 0, piece, s).start()
+
+    def pump(layer, k):
+        for piece in range(3):
+            for way in range(2):
+                @pl.when(gets(way, k))
+                def _(way=way, piece=piece):
+                    z_copy(layer, way, k, piece, got_block(way, k)).wait_recv()
+                    y_copy(layer, way, k, piece, g).start()
+                if k + 1 < rounds:
+                    @pl.when(sends(way, k + 1))
+                    def _(way=way, piece=piece):
+                        z_copy(layer, way, k + 1, piece, sent_block(way, k + 1)).start()
+
+    def await_y(layer, piece):
+        for k in range(rounds):
+            for way in range(2):
+                @pl.when(gets(way, k))
+                def _(way=way, k=k):
+                    y_copy(layer, way, k, piece, other).wait_recv()
+
+    def ag_copy(layer, which, block, target):
+        return pltpu.make_async_remote_copy(
+            src_ref=gathered.at[layer, block], dst_ref=gathered.at[layer, block],
+            send_sem=ag_send.at[layer, which], recv_sem=ag_recv.at[layer, which],
+            device_id={"tp": target}, device_id_type=MESH,
+        )
+
+    def start_gather(layer):
+        ag_copy(layer, 0, t, t2).start()
+        ag_copy(layer, 1, t, t1).start()
+
+    def h_copy(layer, way):
+        return pltpu.make_async_remote_copy(
+            src_ref=halo.at[layer, 1], dst_ref=halo.at[layer, 0 if way == 0 else 2],
+            send_sem=h_send.at[layer, way], recv_sem=h_recv.at[layer, way],
+            device_id={"sp": s + 1 if way == 0 else s - 1}, device_id_type=MESH,
+        )
+
+    def rs_copy(layer, which, target):
+        return pltpu.make_async_remote_copy(
+            src_ref=parts.at[layer, target], dst_ref=arrived.at[layer, which],
+            send_sem=rs_send.at[layer, which], recv_sem=rs_recv.at[layer, which],
+            device_id={"tp": target}, device_id_type=MESH,
+        )
+
+    state_load.wait()
+    start_gather(0)
+    own_sends(0)
+
+    half_span = jnp.int32(pool_windows[0] // 2)
+    for group_id in range(1, GROUPS):
+        half_span = jnp.where(t == group_id, pool_windows[group_id] // 2, half_span)
+    shift = GRID_W.bit_length() - 1
+    first_row = s * rows_here
+    out_tok = lax.broadcasted_iota(jnp.int32, (toks, toks), 0)
+    in_tok = lax.broadcasted_iota(jnp.int32, (toks, toks), 1)
+    out_row = first_row + lax.shift_right_logical(out_tok, shift)
+    out_col = lax.bitwise_and(out_tok, GRID_W - 1)
+    in_col = lax.bitwise_and(in_tok, GRID_W - 1)
+    near_col = (in_col >= out_col - half_span) & (in_col < out_col + half_span)
+    for slot in range(3):
+        in_row = first_row + (slot - 1) * rows_here + lax.shift_right_logical(in_tok, shift)
+        inside = (
+            near_col
+            & (in_row >= out_row - half_span) & (in_row < out_row + half_span)
+            & (in_row >= 0) & (in_row < total_rows)
+        )
+        box[slot] = jnp.where(inside, 1.0, 0.0).astype(jnp.bfloat16)
+    tok_at = lax.broadcasted_iota(jnp.int32, counts.shape, 0)
+    row_at = first_row + lax.shift_right_logical(tok_at, shift)
+    col_at = lax.bitwise_and(tok_at, GRID_W - 1)
+    row_counts = jnp.minimum(row_at + half_span, total_rows) - jnp.maximum(row_at - half_span, 0)
+    col_counts = jnp.minimum(col_at + half_span, GRID_W) - jnp.maximum(col_at - half_span, 0)
+    counts[...] = (row_counts * col_counts).astype(jnp.float32)
+
+    @pl.when(s == 0)
+    def _():
+        for layer in range(LAYERS):
+            halo[layer, 0] = jnp.zeros(halo.shape[2:], halo.dtype)
+
+    @pl.when(s == last)
+    def _():
+        for layer in range(LAYERS):
+            halo[layer, 2] = jnp.zeros(halo.shape[2:], halo.dtype)
+
+    for k in range(rounds):
+        pump(0, k)
+
+    def one_layer(layer, _):
+        more = layer + 1 < LAYERS
+
+        @pl.when(more)
+        def _():
+            own_sends(layer + 1)
+
+        ag_copy(layer, 0, t2, t2).wait_recv()
+        ag_copy(layer, 2, t2, t1).start()
+        ag_copy(layer, 1, t1, t1).wait_recv()
+        ag_copy(layer, 2, t3, t1).wait_recv()
+        total = jnp.zeros((toks, 1), jnp.float32)
+        for block in range(tp_count):
+            wide = gathered[layer, block].astype(jnp.float32)
+            total = total + jnp.sum(wide * wide, axis=1, keepdims=True)
+        scale = lax.rsqrt(total / (tp_count * feats) + norm_eps)
+        for block in range(tp_count):
+            cols = slice(block * feats, (block + 1) * feats)
+            wide = gathered[layer, block].astype(jnp.float32)
+            normed[:, cols] = (wide * scale * gain_ref[pl.ds(layer, 1), cols]).astype(jnp.bfloat16)
+
+        @pl.when(more)
+        def _():
+            pump(layer + 1, 0)
+
+        depth = wp.shape[2]
+
+        def project(buf):
+            acc = None
+            for block in range(sp_count):
+                term = jnp.dot(
+                    normed[:, block * depth:(block + 1) * depth], buf[layer, block],
+                    preferred_element_type=jnp.float32,
+                )
+                acc = term if acc is None else acc + term
+            return acc
+
+        await_y(layer, 0)
+        halo[layer, 1] = project(wp).astype(jnp.bfloat16)
+
+        @pl.when(s < last)
+        def _():
+            h_copy(layer, 0).start()
+
+        @pl.when(s > 0)
+        def _():
+            h_copy(layer, 1).start()
+
+        await_y(layer, 1)
+        gate_buf[...] = jax.nn.sigmoid(project(wg))
+
+        @pl.when(more)
+        def _():
+            pump(layer + 1, 1)
+
+        @pl.when(s > 0)
+        def _():
+            h_copy(layer, 0).wait_recv()
+
+        @pl.when(s < last)
+        def _():
+            h_copy(layer, 1).wait_recv()
+
+        sums = jnp.zeros(counts.shape, jnp.float32)
+        for slot in range(3):
+            sums = sums + jnp.dot(box[slot], halo[layer, slot], preferred_element_type=jnp.float32)
+        pooled = (sums / counts[...] - halo[layer, 1].astype(jnp.float32)).astype(jnp.bfloat16)
+        await_y(layer, 2)
+        for which, target in ((1, t3), (0, t2), (2, t1), (None, t)):
+            parts[layer, target] = jnp.dot(
+                pooled, wb[layer, target], preferred_element_type=jnp.float32
+            ).astype(jnp.bfloat16)
+            if which is not None:
+                rs_copy(layer, which, target).start()
+
+        @pl.when(more)
+        def _():
+            pump(layer + 1, 2)
+
+        branch = parts[layer, t].astype(jnp.float32)
+        for which in (2, 0, 1):
+            rs_copy(layer, which, t1).wait_recv()
+            branch = branch + arrived[layer, which].astype(jnp.float32)
+        state = (gathered[layer, t].astype(jnp.float32) + gate_buf[...] * branch).astype(jnp.bfloat16)
+
+        @pl.when(more)
+        def _():
+            gathered[layer + 1, t] = state
+            start_gather(layer + 1)
+
+        @pl.when(layer + 1 == LAYERS)
+        def _():
+            out_ref[...] = state
+
+        return 0
+
+    lax.fori_loop(0, LAYERS, one_layer, 0)
+
+    def drain(layer, _):
+        for piece in range(3):
+            for k in range(rounds):
+                for way in range(2):
+                    @pl.when(sends(way, k))
+                    def _(way=way, k=k, piece=piece):
+                        z_copy(layer, way, k, piece, sent_block(way, k)).wait_send()
+
+                    @pl.when(gets(way, k))
+                    def _(way=way, k=k, piece=piece):
+                        y_copy(layer, way, k, piece, g).wait_send()
+        ag_copy(layer, 0, t, t2).wait_send()
+        ag_copy(layer, 1, t, t1).wait_send()
+        ag_copy(layer, 2, t2, t1).wait_send()
+
+        @pl.when(s < last)
+        def _():
+            h_copy(layer, 0).wait_send()
+
+        @pl.when(s > 0)
+        def _():
+            h_copy(layer, 1).wait_send()
+
+        rs_copy(layer, 0, t2).wait_send()
+        rs_copy(layer, 1, t3).wait_send()
+        rs_copy(layer, 2, t1).wait_send()
+        return 0
+
+    lax.fori_loop(0, LAYERS, drain, 0)
+
+
+def fused(tokens_in, norm_gain, w_pool_in, w_gate, w_back):
+    sp_count, tp_count = lax.axis_size("sp"), lax.axis_size("tp")
+    toks, feats = tokens_in.shape
+    _, depth, local_pool = w_pool_in.shape
+    rounds = sp_count - 1
+    bf, f32 = jnp.bfloat16, jnp.float32
+    dma = pltpu.SemaphoreType.DMA
+    streams = dma((LAYERS, 2, rounds, 3))
+    return pl.pallas_call(
+        functools.partial(fused_kernel, sp_count, tp_count),
+        out_shape=jax.ShapeDtypeStruct((toks, feats), bf),
+        in_specs=[
+            pl.BlockSpec(memory_space=pltpu.HBM),
+            pl.BlockSpec(memory_space=pltpu.VMEM),
+            pl.BlockSpec(memory_space=pltpu.HBM),
+            pl.BlockSpec(memory_space=pltpu.HBM),
+            pl.BlockSpec(memory_space=pltpu.HBM),
+        ],
+        out_specs=pl.BlockSpec(memory_space=pltpu.VMEM),
+        scratch_shapes=[
+            pltpu.VMEM((LAYERS, sp_count) + w_pool_in.shape[1:], bf),
+            pltpu.VMEM((LAYERS, sp_count) + w_gate.shape[1:], bf),
+            pltpu.VMEM((LAYERS, sp_count) + w_back.shape[1:], bf),
+            pltpu.VMEM((LAYERS, tp_count, toks, feats), bf),
+            pltpu.VMEM((toks, tp_count * feats), bf),
+            pltpu.VMEM((LAYERS, 3, toks, local_pool), bf),
+            pltpu.VMEM((toks, feats), f32),
+            pltpu.VMEM((3, toks, toks), bf),
+            pltpu.VMEM((toks, local_pool), f32),
+            pltpu.VMEM((LAYERS, tp_count, toks, feats), bf),
+            pltpu.VMEM((LAYERS, 3, toks, feats), bf),
+            dma((LAYERS + 1, 3)),
+            streams, streams, streams, streams,
+            dma((LAYERS, 3)), dma((LAYERS, 3)),
+            dma((LAYERS, 2)), dma((LAYERS, 2)),
+            dma((LAYERS, 3)), dma((LAYERS, 3)),
+        ],
+        compiler_params=pltpu.CompilerParams(
+            collective_id=0, has_side_effects=True, vmem_limit_bytes=56 * 1024 * 1024
+        ),
+    )(tokens_in, norm_gain, w_pool_in, w_gate, w_back)
+
+
+def dispatch(tokens_in, norm_gain, w_pool_in, w_gate, w_back):
+    fits = (
+        lax.axis_size("grp") == 2
+        and lax.axis_size("tp") == GROUPS == 4
+        and lax.axis_size("sp") == lax.axis_size("tp")
+        and w_pool_in.shape[2] * GROUPS == POOL_WIDTH
+        and w_pool_in.shape[1] == tokens_in.shape[1]
+        and tokens_in.shape[0] // GRID_W >= max(pool_windows) // 2
+    )
+    step = fused if fits else on_device
+    return step(tokens_in, norm_gain, w_pool_in, w_gate, w_back)
+
+
 def solution(mesh):
     return jax.shard_map(
-        on_device,
+        dispatch,
         mesh=mesh,
         in_specs=(
             P(("grp", "sp"), "tp"),

time: 392 us -> 144 us (0.37)
  waiting for transfers between devices: 261 us -> 0 us
  Pallas kernels: 0 us -> 140 us
  blocking collectives: 48.8 us -> 0 us
  starting transfers between devices: 25.1 us -> 0 us
  matrix products: 16.9 us -> 0 us
  between operations: 14.2 us -> 0.01 us
  local copies, waits for them, and re-layouts: 15.8 us -> 1.67 us
  other arithmetic: 8.76 us -> 0 us
    all_gather x12 -> x0, waiting for transfers between devices: 258 us -> none  [the longest x3 83.9 us: on_device(): lax.all_gather(w_pool_in[layer_id], 'sp', axis=0, tiled=True)]
    pallas_call x0 -> x1, Pallas kernels: none -> 140 us  [fused(): pl.pallas_call(functools.partial(fused_kernel, sp_count, tp_count), out_s...]
    all_gather x3 -> x0, blocking collectives: 48.8 us -> none  [on_device(): full_pooled = lax.all_gather(pooled, 'tp', axis=1, tiled=True)]
    dot_general x9 -> x0, matrix products: 16.9 us -> none  [the longest x3 9.41 us: on_device(): jnp.dot(normed, lax.all_gather(w_gate[layer_id], 'sp', axis=0, tiled=True...]
    ppermute x6 -> x0, starting transfers between devices: 13.9 us -> none  [the longest x3 10.1 us: padded_2(): before = lax.ppermute(last, axis, up)]
    all_to_all x3 -> x0, starting transfers between devices: 10.7 us -> none  [on_device(): lax.all_to_all(back_rows, 'tp', split_axis=1, concat_axis=0, tiled=True)]
    all_to_all x3 -> x0, local copies, waits for them, and re-layouts: 6.82 us -> none  [on_device(): lax.all_to_all(back_rows, 'tp', split_axis=1, concat_axis=0, tiled=True)]
    slice x4 -> x0, local copies, waits for them, and re-layouts: 4.76 us -> none  [the longest x1 2.16 us: on_device(): w_pool_in[layer_id]]
  transfers between devices with their start and end apart: 21 -> 0, of which waited for: 12 -> 0; matrix products, arithmetic and copies ran while one was open for 8% -> 0% of each run, Pallas kernels for 0% -> 0%
where the time goes in v1:
time: 144 us; the launch traced here: 142 us
  Pallas kernels  140 us (97%)
  local copies, waits for them, and re-layouts  1.67 us (1%)
    pallas_call x1, Pallas kernels, fused(): pl.pallas_call(functools.partial(fused_kernel, sp_count, tp_count), out_s...  140 us

profile of v1, /device:TPU:0, one launch (start us, length us, event | category | flops | bytes accessed | tf_op | source)
XLA Modules:
  0.0 141.8 jit_solution(5181107888422055417)
XLA Ops:
  0.0 140.1 %shard_map.55 = bf16[256,512]{1,0:T(8,128)(2,1)} custom-call(bf16[256,512]{1,0:T(8,128)(2,1)} %tok_hbm.1, f32[3,2048]{1,0:T(4,128)} %gain_ref.1, bf16[3,512,256]{2,1,0:T(8,128)(2,1)} %wp_hbm.1, bf16[3,512,512]{2,1,0:T(8,128)(2,1)} %wg_hbm.1, bf16[3,256,512]{2,1,0:T(8,128)(2,1)} %wb_hbm.1), custom_call_target="tpu_custom_call" | custom-call | tf_op jit(solution)/shard_map/pallas_call | solution.py:437
  140.2 1.7 %copy.7 = bf16[256,512]{1,0:T(8,128)(2,1)} copy(bf16[256,512]{1,0:T(8,128)(2,1)} %shard_map.55) | data formatting | bytes 524288

commit v2 on v1

--- a/solution.py
+++ b/solution.py
@@ -114,6 +114,7 @@
 
 
 MESH = pl.DeviceIdType.MESH
+POOL, GATE, BACK = range(3)
 
 
 def halves(buffers, layer, block, half):
@@ -202,25 +203,23 @@
             device_id={"grp": other}, device_id_type=MESH,
         )
 
-    def own_sends(layer):
-        for piece in range(3):
-            load(layer, piece).wait()
-            for way in range(2):
-                @pl.when(sends(way, 0))
-                def _(way=way, piece=piece):
-                    z_copy(layer, way, 0, piece, s).start()
-
-    def pump(layer, k):
-        for piece in range(3):
-            for way in range(2):
-                @pl.when(gets(way, k))
-                def _(way=way, piece=piece):
-                    z_copy(layer, way, k, piece, got_block(way, k)).wait_recv()
-                    y_copy(layer, way, k, piece, g).start()
-                if k + 1 < rounds:
-                    @pl.when(sends(way, k + 1))
-                    def _(way=way, piece=piece):
-                        z_copy(layer, way, k + 1, piece, sent_block(way, k + 1)).start()
+    def own_sends(layer, piece):
+        load(layer, piece).wait()
+        for way in range(2):
+            @pl.when(sends(way, 0))
+            def _(way=way):
+                z_copy(layer, way, 0, piece, s).start()
+
+    def pump(layer, piece, k):
+        for way in range(2):
+            @pl.when(gets(way, k))
+            def _(way=way):
+                z_copy(layer, way, k, piece, got_block(way, k)).wait_recv()
+                y_copy(layer, way, k, piece, g).start()
+            if k + 1 < rounds:
+                @pl.when(sends(way, k + 1))
+                def _(way=way):
+                    z_copy(layer, way, k + 1, piece, sent_block(way, k + 1)).start()
 
     def await_y(layer, piece):
         for k in range(rounds):
@@ -256,7 +255,8 @@
 
     state_load.wait()
     start_gather(0)
-    own_sends(0)
+    own_sends(0, POOL)
+    own_sends(0, BACK)
 
     half_span = jnp.int32(pool_windows[0] // 2)
     for group_id in range(1, GROUPS):
@@ -295,15 +295,12 @@
             halo[layer, 2] = jnp.zeros(halo.shape[2:], halo.dtype)
 
     for k in range(rounds):
-        pump(0, k)
+        pump(0, POOL, k)
 
     def one_layer(layer, _):
         more = layer + 1 < LAYERS
 
-        @pl.when(more)
-        def _():
-            own_sends(layer + 1)
-
+        own_sends(layer, GATE)
         ag_copy(layer, 0, t2, t2).wait_recv()
         ag_copy(layer, 2, t2, t1).start()
         ag_copy(layer, 1, t1, t1).wait_recv()
@@ -318,10 +315,8 @@
             wide = gathered[layer, block].astype(jnp.float32)
             normed[:, cols] = (wide * scale * gain_ref[pl.ds(layer, 1), cols]).astype(jnp.bfloat16)
 
-        @pl.when(more)
-        def _():
-            pump(layer + 1, 0)
-
+        for k in range(rounds - 1):
+            pump(layer, BACK, k)
         depth = wp.shape[2]
 
         def project(buf):
@@ -334,7 +329,7 @@
                 acc = term if acc is None else acc + term
             return acc
 
-        await_y(layer, 0)
+        await_y(layer, POOL)
         halo[layer, 1] = project(wp).astype(jnp.bfloat16)
 
         @pl.when(s < last)
@@ -345,12 +340,13 @@
         def _():
             h_copy(layer, 1).start()
 
-        await_y(layer, 1)
-        gate_buf[...] = jax.nn.sigmoid(project(wg))
+        pump(layer, BACK, rounds - 1)
 
         @pl.when(more)
         def _():
-            pump(layer + 1, 1)
+            own_sends(layer + 1, POOL)
+
+        pump(layer, GATE, 0)
 
         @pl.when(s > 0)
         def _():
@@ -364,7 +360,7 @@
         for slot in range(3):
             sums = sums + jnp.dot(box[slot], halo[layer, slot], preferred_element_type=jnp.float32)
         pooled = (sums / counts[...] - halo[layer, 1].astype(jnp.float32)).astype(jnp.bfloat16)
-        await_y(layer, 2)
+        await_y(layer, BACK)
         for which, target in ((1, t3), (0, t2), (2, t1), (None, t)):
             parts[layer, target] = jnp.dot(
                 pooled, wb[layer, target], preferred_element_type=jnp.float32
@@ -372,10 +368,17 @@
             if which is not None:
                 rs_copy(layer, which, target).start()
 
+        for k in range(1, rounds):
+            pump(layer, GATE, k)
+
         @pl.when(more)
         def _():
-            pump(layer + 1, 2)
-
+            own_sends(layer + 1, BACK)
+            for k in range(rounds - 1):
+                pump(layer + 1, POOL, k)
+
+        await_y(layer, GATE)
+        gate_buf[...] = jax.nn.sigmoid(project(wg))
         branch = parts[layer, t].astype(jnp.float32)
         for which in (2, 0, 1):
             rs_copy(layer, which, t1).wait_recv()
@@ -386,6 +389,7 @@
         def _():
             gathered[layer + 1, t] = state
             start_gather(layer + 1)
+            pump(layer + 1, POOL, rounds - 1)
 
         @pl.when(layer + 1 == LAYERS)
         def _():

time: 144 us -> 134 us (0.931); the launches traced: 142 us -> 134 us
  Pallas kernels: 140 us -> 132 us
    pallas_call x1, Pallas kernels: 140 us -> 132 us  [fused(): pl.pallas_call(functools.partial(fused_kernel, sp_count, tp_count), out_s...]
where the time goes in v2:
time: 134 us
  Pallas kernels  132 us (99%)
  local copies, waits for them, and re-layouts  1.67 us (1%)
    pallas_call x1, Pallas kernels, fused(): pl.pallas_call(functools.partial(fused_kernel, sp_count, tp_count), out_s...  132 us

profile of v2, /device:TPU:0, one launch (start us, length us, event | category | flops | bytes accessed | tf_op | source)
XLA Modules:
  0.0 133.7 jit_solution(17793579418156387487)
XLA Ops:
  0.0 132.0 %shard_map.55 = bf16[256,512]{1,0:T(8,128)(2,1)} custom-call(bf16[256,512]{1,0:T(8,128)(2,1)} %tok_hbm.1, f32[3,2048]{1,0:T(4,128)} %gain_ref.1, bf16[3,512,256]{2,1,0:T(8,128)(2,1)} %wp_hbm.1, bf16[3,512,512]{2,1,0:T(8,128)(2,1)} %wg_hbm.1, bf16[3,256,512]{2,1,0:T(8,128)(2,1)} %wb_hbm.1), custom_call_target="tpu_custom_call" | custom-call | tf_op jit(solution)/shard_map/pallas_call | solution.py:441
  132.1 1.7 %copy.7 = bf16[256,512]{1,0:T(8,128)(2,1)} copy(bf16[256,512]{1,0:T(8,128)(2,1)} %shard_map.55) | data formatting | bytes 524288

commit v3 on v2

--- a/solution.py
+++ b/solution.py
@@ -300,6 +300,7 @@
     def one_layer(layer, _):
         more = layer + 1 < LAYERS
 
+        pump(layer, BACK, 0)
         own_sends(layer, GATE)
         ag_copy(layer, 0, t2, t2).wait_recv()
         ag_copy(layer, 2, t2, t1).start()
@@ -315,7 +316,7 @@
             wide = gathered[layer, block].astype(jnp.float32)
             normed[:, cols] = (wide * scale * gain_ref[pl.ds(layer, 1), cols]).astype(jnp.bfloat16)
 
-        for k in range(rounds - 1):
+        for k in range(1, rounds - 1):
             pump(layer, BACK, k)
         depth = wp.shape[2]
 
@@ -342,11 +343,12 @@
 
         pump(layer, BACK, rounds - 1)
 
+        pump(layer, GATE, 0)
+
         @pl.when(more)
         def _():
             own_sends(layer + 1, POOL)
 
-        pump(layer, GATE, 0)
 
         @pl.when(s > 0)
         def _():
@@ -373,8 +375,9 @@
 
         @pl.when(more)
         def _():
+            pump(layer + 1, POOL, 0)
             own_sends(layer + 1, BACK)
-            for k in range(rounds - 1):
+            for k in range(1, rounds - 1):
                 pump(layer + 1, POOL, k)
 
         await_y(layer, GATE)

time: 134 us -> 131 us (0.978)
  Pallas kernels: 132 us -> 129 us
    pallas_call x1, Pallas kernels: 132 us -> 129 us  [fused(): pl.pallas_call(functools.partial(fused_kernel, sp_count, tp_count), out_s...]
where the time goes in v3:
time: 131 us
  Pallas kernels  129 us (98%)
  local copies, waits for them, and re-layouts  1.67 us (1%)
    pallas_call x1, Pallas kernels, fused(): pl.pallas_call(functools.partial(fused_kernel, sp_count, tp_count), out_s...  129 us

profile of v3, /device:TPU:0, one launch (start us, length us, event | category | flops | bytes accessed | tf_op | source)
XLA Modules:
  0.0 130.9 jit_solution(12084254394706787641)
XLA Ops:
  0.0 129.2 %shard_map.55 = bf16[256,512]{1,0:T(8,128)(2,1)} custom-call(bf16[256,512]{1,0:T(8,128)(2,1)} %tok_hbm.1, f32[3,2048]{1,0:T(4,128)} %gain_ref.1, bf16[3,512,256]{2,1,0:T(8,128)(2,1)} %wp_hbm.1, bf16[3,512,512]{2,1,0:T(8,128)(2,1)} %wg_hbm.1, bf16[3,256,512]{2,1,0:T(8,128)(2,1)} %wb_hbm.1), custom_call_target="tpu_custom_call" | custom-call | tf_op jit(solution)/shard_map/pallas_call | solution.py:444
  129.2 1.7 %copy.7 = bf16[256,512]{1,0:T(8,128)(2,1)} copy(bf16[256,512]{1,0:T(8,128)(2,1)} %shard_map.55) | data formatting | bytes 524288

commit v4 on v3

--- a/solution.py
+++ b/solution.py
@@ -301,9 +301,9 @@
         more = layer + 1 < LAYERS
 
         pump(layer, BACK, 0)
-        own_sends(layer, GATE)
         ag_copy(layer, 0, t2, t2).wait_recv()
         ag_copy(layer, 2, t2, t1).start()
+        own_sends(layer, GATE)
         ag_copy(layer, 1, t1, t1).wait_recv()
         ag_copy(layer, 2, t3, t1).wait_recv()
         total = jnp.zeros((toks, 1), jnp.float32)
@@ -362,6 +362,7 @@
         for slot in range(3):
             sums = sums + jnp.dot(box[slot], halo[layer, slot], preferred_element_type=jnp.float32)
         pooled = (sums / counts[...] - halo[layer, 1].astype(jnp.float32)).astype(jnp.bfloat16)
+        pump(layer, GATE, 1)
         await_y(layer, BACK)
         for which, target in ((1, t3), (0, t2), (2, t1), (None, t)):
             parts[layer, target] = jnp.dot(
@@ -370,7 +371,7 @@
             if which is not None:
                 rs_copy(layer, which, target).start()
 
-        for k in range(1, rounds):
+        for k in range(2, rounds):
             pump(layer, GATE, k)
 
         @pl.when(more)

time: 131 us -> 131 us (level)
  no operation moved by 1% of the time
where the time goes in v4:
time: 131 us
  Pallas kernels  129 us (98%)
  local copies, waits for them, and re-layouts  1.67 us (1%)
    pallas_call x1, Pallas kernels, fused(): pl.pallas_call(functools.partial(fused_kernel, sp_count, tp_count), out_s...  129 us

profile of v4, /device:TPU:0, one launch (start us, length us, event | category | flops | bytes accessed | tf_op | source)
XLA Modules:
  0.0 130.9 jit_solution(7706428976830543131)
XLA Ops:
  0.0 129.2 %shard_map.55 = bf16[256,512]{1,0:T(8,128)(2,1)} custom-call(bf16[256,512]{1,0:T(8,128)(2,1)} %tok_hbm.1, f32[3,2048]{1,0:T(4,128)} %gain_ref.1, bf16[3,512,256]{2,1,0:T(8,128)(2,1)} %wp_hbm.1, bf16[3,512,512]{2,1,0:T(8,128)(2,1)} %wg_hbm.1, bf16[3,256,512]{2,1,0:T(8,128)(2,1)} %wb_hbm.1), custom_call_target="tpu_custom_call" | custom-call | tf_op jit(solution)/shard_map/pallas_call | solution.py:445
  129.3 1.7 %copy.7 = bf16[256,512]{1,0:T(8,128)(2,1)} copy(bf16[256,512]{1,0:T(8,128)(2,1)} %shard_map.55) | data formatting | bytes 524288
